TPU v7x, 32 devices: a whole 2x2x4 slice. The times are simulated.
32 devices in a mesh: sp: 8 (over z, x), tp: 4 (over y, core).
Axes of the slice: x: 2, y: 2, z: 4, core: 2. Of those that a mesh axis runs over, the one named last changes fastest.
Arguments:
- queries: bfloat16 [2048, 2048], P('sp', 'tp'), may hold values from -6 to 6
- keys: bfloat16 [2048, 1024], P('sp', 'tp'), may hold values from -6 to 6
- values: bfloat16 [2048, 1024], P('sp', 'tp'), may hold values from -6 to 6
- docs: int32 [2048], P('sp'), may hold values from 0 to 2, never falling along the last dimension, each value on 1 to 1280 neighbouring positions
- query_gain: float32 [64], replicated, may hold values from 0.5 to 8
- key_gain: float32 [64], replicated, may hold values from 0.5 to 8
- out_weight: bfloat16 [2048, 2048], P('tp'), may hold values from -0.125 to 0.125
- residual: bfloat16 [2048, 2048], P('sp', 'tp'), may hold values from -12 to 12
- norm_gain: float32 [2048], P('tp'), may hold values from 0.1 to 1.9
- routes: int32 [2048, 2], P('sp'), may hold values from 0 to 7, all different within a row; in each aligned block of 256 rows (0 to 255, 256 to 511, ...) at most 80 rows name the same one
- route_weight: float32 [2048, 2], P('sp'), may hold values from 0.1 to 1
- gate_weight: bfloat16 [8, 2048, 4096], P('sp', None, 'tp'), may hold values from -0.3125 to 0.3125
- up_weight: bfloat16 [8, 2048, 4096], P('sp', None, 'tp'), may hold values from -0.3125 to 0.3125
- down_weight: bfloat16 [8, 4096, 2048], P('sp', 'tp'), may hold values from -0.09375 to 0.09375
Outputs:
- mixed: bfloat16 [2048, 2048], P('sp', 'tp')
Inputs may be any that keep to these rules, and one draw needn't show every extreme that they name: `routes`: in each aligned block of 256 rows no expert is named by more than 80 rows, and 80 is reached in some block; a row names 2 different experts. `docs`: document numbers never fall along the sequence; a document holds at most 1280 positions.
All inputs are finite; a program needn't handle non-finite values.
Results may differ from a plain program's by a relative error of at most 0.028.
The roundings to bfloat16 on the way count: a program that leaves them out, or rounds other values in their place, can miss the bound.
Values may be sent and summed in bfloat16 or wider, within the bound.
A program may use at most 64 MiB of HBM per device.

v0:
```python
import jax
import jax.numpy as jnp
from jax import lax
from jax.sharding import PartitionSpec as P

GRID_W = 64
EPSILON = 1e-06
NEG_BIG = -1e30
ROTARY_BASE = 10000.0
CLAMP_LIMIT = 7.0
SIGMOID_SCALE = 1.702


def rope_tables(positions, head_dim):
    quarter = head_dim // 4
    freqs = ROTARY_BASE ** (-jnp.arange(quarter, dtype=jnp.float32) / quarter)
    row_pos = (positions // GRID_W).astype(jnp.float32)
    col_pos = (positions % GRID_W).astype(jnp.float32)
    angle = jnp.concatenate([row_pos[:, None] * freqs, col_pos[:, None] * freqs], axis=1)
    return (jnp.cos(angle), jnp.sin(angle))


def norm_rotate(heads, gain, cosine_table, sine_table):
    entries = heads.astype(jnp.float32)
    entries = (
        entries * lax.rsqrt(jnp.mean(entries * entries, axis=-1, keepdims=True) + EPSILON) * gain
    )
    pairs = entries.reshape(entries.shape[:-1] + (entries.shape[-1] // 2, 2))
    first = pairs[..., 0]
    second = pairs[..., 1]
    cos_rows = cosine_table[:, None, :]
    sin_rows = sine_table[:, None, :]
    turned = jnp.stack(
        [first * cos_rows - second * sin_rows, first * sin_rows + second * cos_rows], axis=-1
    )
    return turned.reshape(heads.shape).astype(jnp.bfloat16)


def clamped_unit(gate_pre, up_pre):
    bounded = jnp.minimum(gate_pre, CLAMP_LIMIT)
    linear = jnp.clip(up_pre, -CLAMP_LIMIT, CLAMP_LIMIT)
    return (bounded * jax.nn.sigmoid(SIGMOID_SCALE * bounded) * (linear + 1.0)).astype(jnp.bfloat16)


def block_length(length):
    block_size = length
    while block_size > 2048 and block_size % 2 == 0:
        block_size = block_size // 2
    return block_size


def softmax_update(running, inputs, query_rot, own_tags, score_scale):
    row_peak, denominator, carried = running
    key_block, value_block, tag_block = inputs
    scores = (
        jnp.einsum("tkgd,pkd->tkgp", query_rot, key_block, preferred_element_type=jnp.float32)
        * score_scale
    )
    allowed = own_tags[:, None, None, None] == tag_block[None, None, None, :]
    scores = jnp.where(allowed, scores, NEG_BIG)
    new_peak = jnp.maximum(row_peak, jnp.max(scores, axis=-1))
    weights = jnp.where(allowed, jnp.exp(scores - new_peak[..., None]), 0.0)
    factor = jnp.exp(row_peak - new_peak)
    denominator = denominator * factor + jnp.sum(weights, axis=-1)
    carried = carried * factor[..., None] + jnp.einsum(
        "tkgp,pkd->tkgd",
        weights.astype(jnp.bfloat16),
        value_block,
        preferred_element_type=jnp.float32,
    )
    return (new_peak, denominator, carried)


def per_device(
    queries,
    keys,
    values,
    docs,
    query_gain,
    key_gain,
    out_weight,
    residual,
    norm_gain,
    routes,
    route_weight,
    gate_weight,
    up_weight,
    down_weight,
):
    tokens = queries.shape[0]
    head_dim = query_gain.shape[0]
    query_heads = queries.shape[1] // head_dim
    pair_heads = keys.shape[1] // head_dim
    pair_width = keys.shape[1]
    positions = lax.axis_index("sp") * tokens + jnp.arange(tokens, dtype=jnp.int32)
    cosine_table, sine_table = rope_tables(positions, head_dim)
    query_rot = norm_rotate(
        queries.reshape(tokens, query_heads, head_dim), query_gain, cosine_table, sine_table
    )
    query_rot = query_rot.reshape(tokens, pair_heads, 2, head_dim)
    key_rot = norm_rotate(
        keys.reshape(tokens, pair_heads, head_dim), key_gain, cosine_table, sine_table
    )
    stacked = jnp.concatenate([key_rot.reshape(tokens, pair_width), values], axis=1)
    own_tags = docs.astype(jnp.bfloat16)
    score_scale = head_dim ** (-0.5)
    stat_shape = (tokens, pair_heads, 2)
    initial = (
        jnp.full(stat_shape, NEG_BIG, jnp.float32),
        jnp.zeros(stat_shape, jnp.float32),
        jnp.zeros(stat_shape + (head_dim,), jnp.float32),
    )
    pair_rows = lax.all_gather(stacked, "sp", axis=0, tiled=True)
    tag_rows = lax.all_gather(own_tags, "sp", axis=0, tiled=True)
    length = pair_rows.shape[0]
    block_size = block_length(length)
    blocks = length // block_size
    key_part = pair_rows[:, :pair_width].reshape(blocks, block_size, pair_heads, head_dim)
    value_part = pair_rows[:, pair_width:].reshape(blocks, block_size, pair_heads, head_dim)
    tag_part = tag_rows.reshape(blocks, block_size)

    def advance(carry_state, inputs):
        return (softmax_update(carry_state, inputs, query_rot, own_tags, score_scale), None)

    result, _ = lax.scan(advance, initial, (key_part, value_part, tag_part))
    row_peak, denominator, carried = result
    attended = (
        (carried / denominator[..., None])
        .astype(jnp.bfloat16)
        .reshape(tokens, query_heads * head_dim)
    )
    width_local = residual.shape[1]
    projected = lax.psum_scatter(
        lax.dot_general(
            out_weight, attended, (((0,), (1,)), ((), ())), preferred_element_type=jnp.float32
        ).astype(jnp.bfloat16),
        "tp",
        scatter_dimension=0,
        tiled=True,
    ).astype(jnp.float32)
    mixed_first = residual.astype(jnp.float32) + projected.T
    squares = lax.psum(jnp.sum(mixed_first * mixed_first, axis=1), "tp")
    full_width = width_local * lax.axis_size("tp")
    normed = (mixed_first * lax.rsqrt(squares / full_width + EPSILON)[:, None] * norm_gain).astype(
        jnp.bfloat16
    )
    experts = lax.axis_size("sp")
    top_count = routes.shape[1]
    capacity = max(2, 5 * tokens * top_count // (4 * experts))
    flat_routes = routes.reshape(-1)
    entries = flat_routes.shape[0]
    expert_ids = jnp.arange(experts, dtype=jnp.int32)
    onehot = (flat_routes[:, None] == expert_ids[None, :]).astype(jnp.int32)
    earlier = jnp.cumsum(onehot, axis=0) - onehot
    slot_index = jnp.sum(earlier * onehot, axis=1)
    slot_ids = jnp.arange(capacity, dtype=jnp.int32)
    matches = (flat_routes[:, None, None] == expert_ids[None, :, None]) & (
        slot_index[:, None, None] == slot_ids[None, None, :]
    )
    entry_ids = jnp.arange(entries, dtype=jnp.int32)
    source_entry = jnp.sum(jnp.where(matches, entry_ids[:, None, None], 0), axis=0)
    occupied = jnp.any(matches, axis=0)
    source_row = source_entry // top_count
    gate_local = gate_weight[0]
    up_local = up_weight[0]
    down_local = down_weight[0]
    model_width = gate_local.shape[0]
    outgoing = jnp.where(occupied[..., None], normed[source_row], jnp.zeros((), jnp.bfloat16))
    arrived = lax.all_to_all(outgoing, "sp", split_axis=0, concat_axis=0, tiled=True)
    sources = arrived.shape[0]
    flat_rows = arrived.reshape(-1, width_local)
    column_piece = lax.all_gather(flat_rows, "tp", axis=1, tiled=True)
    gate_pre = jnp.dot(column_piece, gate_local, preferred_element_type=jnp.float32)
    up_pre = jnp.dot(column_piece, up_local, preferred_element_type=jnp.float32)
    hidden = clamped_unit(gate_pre, up_pre)
    partial_value = jnp.dot(hidden, down_local, preferred_element_type=jnp.float32).reshape(
        sources, capacity, model_width
    )
    expert_out = lax.psum_scatter(
        partial_value.astype(jnp.bfloat16), "tp", scatter_dimension=2, tiled=True
    )
    returned = lax.all_to_all(expert_out, "sp", split_axis=0, concat_axis=0, tiled=True)
    lookup = flat_routes * capacity + slot_index
    picked = (
        returned.reshape(-1, width_local)[lookup]
        .reshape(tokens, top_count, width_local)
        .astype(jnp.float32)
    )
    routed = jnp.sum(route_weight[:, :, None] * picked, axis=1)
    return (mixed_first + routed).astype(jnp.bfloat16)


def solution(mesh):
    in_specs = (
        P("sp", "tp"),
        P("sp", "tp"),
        P("sp", "tp"),
        P("sp"),
        P(),
        P(),
        P("tp", None),
        P("sp", "tp"),
        P("tp"),
        P("sp", None),
        P("sp", None),
        P("sp", None, "tp"),
        P("sp", None, "tp"),
        P("sp", "tp", None),
    )
    out_specs = P("sp", "tp")
    return jax.shard_map(
        per_device, mesh=mesh, in_specs=in_specs, out_specs=out_specs, check_vma=False
    )
```

profile of v0, /device:TPU:0, one launch (start us, length us, event | category | flops | bytes accessed | tf_op | source)
XLA Modules:
  0.0 244.0 jit_solution(5147437151146860078)
XLA Ops:
  6.5 1.2 copy.40
  7.9 1.0 copy.41
  8.9 0.8 mul.239
  10.8 0.7 pad_maximum_fusion
  11.6 0.7 convert_element_type.90
  12.3 22.4 %all-gather = bf16[8,1,256]{2,1,0:T(2,128)(2,1)S(1)} all-gather(bf16[1,1,256]{2,1,0:T(2,128)(2,1)S(1)} %reshape.382), channel_id=1, replica_groups=mesh['sp'=8,'tp'=4] {'sp'}, dimensions={0}, use_global_device_ids=true | all-gather | bytes 4608 | tf_op jit(solution)/shard_map/all_gather | solution.py:114
  34.7 1.1 copy.42
  36.6 0.7 subtract_convert_fusion
  38.4 26.5 %all-gather.4.cloned.1.call-done = bf16[2048,512]{0,1:T(8,128)(2,1)} async-done(((bf16[256,512]{0,1:T(8,128)(2,1)}), bf16[2048,512]{0,1:T(8,128)(2,1)}) %all-gather.4.cloned.1.call-update) | async-done | bytes 2097168 | tf_op jit(solution)/shard_map/all_gather | solution.py:113
  64.8 1.7 fusion.46
  66.5 2.6 %fusion = (f32[256,4,2]{0,2,1:T(2,128)S(1)}, f32[4,2048,256,2]{2,1,3,0:T(8,128)S(1)}) fusion(pred[256,2048]{0,1:T(8,128)(4,1)S(1)} %broadcast_compare_fusion, bf16[2048,4,64,1]{0,2,3,1:T(8,128)(2,1)S(1)} %bitcast.120, bf16[256,4,2,64]{0,3,2,1:T(8,128)(2,1)S(1)} %convert_element_type.100), kind=kOutput, calls=%fused_computation.4 | convolution fusion | flops 549451776 | bytes 18620416 | tf_op jit(solution)/shard_map/while/body/eval_jaxpr/tkgd,pkd->tkgp/dot_general | solution.py:56
  69.1 4.0 %fusion.1 = f32[256,4,2]{0,2,1:T(2,128)S(1)} fusion(f32[4,2048,256,2]{2,1,3,0:T(8,128)S(1)} %get-tuple-element.45, f32[256,4,2]{0,2,1:T(2,128)S(1)} %broadcast_maximum_fusion, pred[256,2048]{0,1:T(8,128)(4,1)S(1)} %broadcast_compare_fusion), kind=kLoop, calls=%fused_computation.5 | loop fusion | flops 20969472 | bytes 17317888 | tf_op jit(solution)/shard_map/while/body/eval_jaxpr/reduce_sum | solution.py:64
  73.2 3.9 %fusion.28 = bf16[256,4,2,64]{0,3,2,1:T(8,128)(2,1)S(1)} fusion(bf16[2048,4,64,1]{0,2,3,1:T(8,128)(2,1)S(1)} %bitcast.119, f32[4,2048,256,2]{2,1,3,0:T(8,128)S(1)} %get-tuple-element.45, f32[256,4,2]{0,2,1:T(2,128)S(1)} %broadcast_maximum_fusion, pred[256,2048]{0,1:T(8,128)(4,1)S(1)} %broadcast_compare_fusion, f32[256,4,2]{0,2,1:T(2,128)S(1)} %get-tuple-element.41, ...), kind=kOutput, calls=%fused_computation.26 | convolution fusion | flops 558235648 | bytes 18636800 | tf_op jit(solution)/shard_map/while/body/eval_jaxpr/tkgp,pkd->tkgd/dot_general | solution.py:65
  77.2 1.7 fusion.15
  79.6 1.1 reduce-window.6
  81.8 20.3 %reduce-scatter.3.cloned.1.call-done = bf16[512,256]{0,1:T(8,128)(2,1)} async-done(((bf16[2048,256]{0,1:T(8,128)(2,1)}), bf16[512,256]{0,1:T(8,128)(2,1)}) %reduce-scatter.3.cloned.1.call-update) | async-done | bytes 262160 | tf_op jit(solution)/shard_map/reduce_scatter | solution.py:133
  102.1 1.1 multiply_reduce_fusion.1
  103.2 5.8 %psum.7 = f32[256]{0:T(256)S(1)} all-reduce(f32[256]{0:T(256)S(1)} %multiply_reduce_fusion.1), channel_id=1, replica_groups=mesh['sp'=8,'tp'=4] {'tp'}, use_global_device_ids=true, to_apply=%region_10.11 | all-reduce | flops 256 | bytes 2048 | tf_op jit(solution)/shard_map/psum | solution.py:142
  109.0 1.1 multiply_convert_fusion.1
  110.1 2.8 %gather_fusion = bf16[640,512]{1,0:T(8,128)(2,1)S(1)} fusion(bf16[256,512]{1,0:T(8,128)(2,1)S(1)} %multiply_convert_fusion.1, s32[1024]{0:T(1024)S(1)} %pad_clamp_fusion.1), kind=kCustom, calls=%fused_computation | custom fusion | bytes 1313280 | tf_op jit(solution)/shard_map/gather | solution.py:168
  113.0 23.1 %all_to_all.10 = bf16[8,80,512]{2,1,0:T(8,128)(2,1)} all-to-all(bf16[8,80,512]{2,1,0:T(8,128)(2,1)S(1)} %broadcast_select_fusion), channel_id=1, replica_groups=mesh['sp'=8,'tp'=4] {'sp'}, dimensions={0} | all-to-all | bytes 1310720 | tf_op jit(solution)/shard_map/all_to_all | solution.py:169
  136.2 23.3 %all-gather.6.cloned.1.call-done = bf16[640,2048]{1,0:T(8,128)(2,1)} async-done(((bf16[640,512]{1,0:T(8,128)(2,1)}), bf16[640,2048]{1,0:T(8,128)(2,1)}) %all-gather.6.cloned.1.call-update) | async-done | bytes 2621456 | tf_op jit(solution)/shard_map/all_gather | solution.py:172
  159.5 5.6 %fusion.8 = f32[640,1024]{1,0:T(8,128)S(1)} fusion(bf16[640,2048]{1,0:T(8,128)(2,1)} %all-gather.6.cloned.1.call-done, bf16[1,2048,1024]{2,1,0:T(8,128)(2,1)} %param.26), kind=kOutput, calls=%fused_computation.11 | convolution fusion | flops 2684354560 | bytes 9437184 | tf_op jit(solution)/shard_map/dot_general | solution.py:174
  165.1 3.5 %multiply_convert_fusion = bf16[640,1024]{1,0:T(8,128)(2,1)S(1)} fusion(f32[640,1024]{1,0:T(8,128)S(1)} %fusion.8, bf16[640,2048]{1,0:T(8,128)(2,1)S(1)} %copy-done.8, bf16[1,2048,1024]{2,1,0:T(8,128)(2,1)S(1)} %copy-done.6), kind=kOutput, calls=%fused_computation.16 | convolution fusion | flops 2690908160 | bytes 10747904 | tf_op jit(solution)/shard_map/dot_general | solution.py:173
  168.7 4.2 %fusion.12 = bf16[8,80,2048]{2,1,0:T(8,128)(2,1)} fusion(bf16[8,80,1024]{2,1,0:T(8,128)(2,1)S(1)} %bitcast.126, bf16[1,1024,2048]{2,1,0:T(8,128)(2,1)S(1)} %copy-done.7), kind=kOutput, calls=%fused_computation.15 | convolution fusion | flops 2685665280 | bytes 8126464 | tf_op jit(solution)/shard_map/dot_general | solution.py:176
  172.9 34.5 %reduce-scatter.5.cloned.1.call-done = bf16[8,80,512]{2,1,0:T(8,128)(2,1)} async-done(((bf16[8,80,2048]{2,1,0:T(8,128)(2,1)}), bf16[8,80,512]{2,1,0:T(8,128)(2,1)}) %reduce-scatter.5.cloned.1.call-update) | async-done | bytes 655376 | tf_op jit(solution)/shard_map/reduce_scatter | solution.py:179
  207.4 5.5 %all-to-all-start.1 = ((bf16[8,80,512]{2,1,0:T(8,128)(2,1)}), bf16[8,80,512]{2,1,0:T(8,128)(2,1)S(1)}, u32[]{:S(2)}, u32[]{:S(2)}) async-start(bf16[8,80,512]{2,1,0:T(8,128)(2,1)} %reduce-scatter.5.cloned.1.call-done), calls=%async_computation.3 | async-start | bytes 1310720 | tf_op jit(solution)/shard_map/all_to_all | solution.py:182
  213.4 16.7 %all-to-all-done.1 = bf16[8,80,512]{2,1,0:T(8,128)(2,1)S(1)} async-done(((bf16[8,80,512]{2,1,0:T(8,128)(2,1)}), bf16[8,80,512]{2,1,0:T(8,128)(2,1)S(1)}, u32[]{:S(2)}, u32[]{:S(2)}) %all-to-all-start.1) | async-done | bytes 655392 | tf_op jit(solution)/shard_map/all_to_all | solution.py:182
  230.0 2.6 %gather_fusion.1 = bf16[512,512]{1,0:T(8,128)(2,1)} fusion(bf16[640,512]{1,0:T(8,128)(2,1)S(1)} %bitcast.116, s32[1024]{0:T(1024)S(1)} %pad_clamp_fusion), kind=kCustom, calls=%fused_computation.1 | custom fusion | bytes 1050624 | tf_op jit(solution)/shard_map/gather | solution.py:185
  232.7 1.7 reshape.364
  234.4 1.3 multiply_reduce_fusion
  235.7 1.8 add_convert_fusion
  (73 shorter events, 5.5 us)
Async XLA Ops:
  6.5 70.7 %copy-start = (bf16[512,2048]{1,0:T(8,128)(2,1)S(1)}, bf16[512,2048]{1,0:T(8,128)(2,1)}, u32[]{:S(2)}) copy-start(bf16[512,2048]{1,0:T(8,128)(2,1)} %param.20) | copy-start | bytes 6291460
  6.5 29.6 %copy-start.5 = (f32[64]{0:T(128)S(1)}, f32[64]{0:T(128)}, u32[]{:S(2)}) copy-start(f32[64]{0:T(128)} %param.18) | copy-start | bytes 772
  6.5 58.3 %all-gather.4.cloned.1.call-start = ((), (), s32[]{:S(2)}) async-start(), calls=%async_computation.4 | async-start | bytes 2359296 | tf_op jit(solution)/shard_map/all_gather | solution.py:113
  11.6 90.5 %reduce-scatter.3.cloned.1.call-start = ((), (), s32[]{:S(2)}) async-start(), calls=%async_computation.5 | async-start | bytes 1310720 | tf_op jit(solution)/shard_map/reduce_scatter | solution.py:133
  77.2 2.0 copy-start.2
  77.2 24.9 %copy-start.1 = (bf16[256,512]{1,0:T(8,128)(2,1)S(1)}, bf16[256,512]{1,0:T(8,128)(2,1)}, u32[]{:S(2)}) copy-start(bf16[256,512]{1,0:T(8,128)(2,1)} %param.21) | copy-start | bytes 786436
  77.2 31.8 %copy-start.3 = (f32[512]{0:T(512)S(1)}, f32[512]{0:T(512)}, u32[]{:S(2)}) copy-start(f32[512]{0:T(512)} %param.22) | copy-start | bytes 6148
  78.9 80.6 %all-gather.6.cloned.1.call-start = ((), (), s32[]{:S(2)}) async-start(), calls=%async_computation.6 | async-start | bytes 3276800 | tf_op jit(solution)/shard_map/all_gather | solution.py:172
  136.1 71.3 %reduce-scatter.5.cloned.1.call-start = ((), (), s32[]{:S(2)}) async-start(), calls=%async_computation.7 | async-start | bytes 3276800 | tf_op jit(solution)/shard_map/reduce_scatter | solution.py:179
  159.5 5.6 %copy-start.6 = (bf16[1,2048,1024]{2,1,0:T(8,128)(2,1)S(1)}, bf16[1,2048,1024]{2,1,0:T(8,128)(2,1)}, u32[]{:S(2)}) copy-start(bf16[1,2048,1024]{2,1,0:T(8,128)(2,1)} %param.25) | copy-start | bytes 12582916
  159.5 5.6 %copy-start.8 = (bf16[640,2048]{1,0:T(8,128)(2,1)S(1)}, bf16[640,2048]{1,0:T(8,128)(2,1)}, u32[]{:S(2)}) copy-start(bf16[640,2048]{1,0:T(8,128)(2,1)} %all-gather.6.cloned.1.call-done) | copy-start | bytes 7864324
  165.1 3.6 %copy-start.7 = (bf16[1,1024,2048]{2,1,0:T(8,128)(2,1)S(1)}, bf16[1,1024,2048]{2,1,0:T(8,128)(2,1)}, u32[]{:S(2)}) copy-start(bf16[1,1024,2048]{2,1,0:T(8,128)(2,1)} %param.27) | copy-start | bytes 12582916
  172.9 40.3 %copy-start.4 = (f32[256,2]{0,1:T(2,128)S(1)}, f32[256,2]{0,1:T(2,128)}, u32[]{:S(2)}) copy-start(f32[256,2]{0,1:T(2,128)} %param.24) | copy-start | bytes 6148
  207.4 22.6 %all-to-all-start.1 = ((bf16[8,80,512]{2,1,0:T(8,128)(2,1)}), bf16[8,80,512]{2,1,0:T(8,128)(2,1)S(1)}, u32[]{:S(2)}, u32[]{:S(2)}) async-start(bf16[8,80,512]{2,1,0:T(8,128)(2,1)} %reduce-scatter.5.cloned.1.call-done), calls=%async_computation.3 | async-start | bytes 1310720 | tf_op jit(solution)/shard_map/all_to_all | solution.py:182
Sparse Core Ops, SparseCore 0:
  11.7 53.0 all-gather.3
  79.1 22.9 reduce-scatter.2
  136.2 23.2 all-gather.5
  173.0 34.3 reduce-scatter.4
where the time goes:
time: 245 us; the launch traced here: 244 us
  waiting for transfers between devices  121 us (49%)
  blocking collectives  51.2 us (21%)
  matrix products  21.6 us (9%)
  other arithmetic  15.9 us (6%)
  local copies, waits for them, and re-layouts  14.6 us (6%)
  between operations  13.6 us (6%)
  starting transfers between devices  5.82 us (2%)
    reduce_scatter x1, waiting for transfers between devices, per_device(): lax.psum_scatter(partial_value.astype(jnp.bfloat16), 'tp', scatter_dimens...  34.5 us
    all_gather x1, waiting for transfers between devices, per_device(): pair_rows = lax.all_gather(stacked, 'sp', axis=0, tiled=True)  26.5 us
    all_gather x1, waiting for transfers between devices, per_device(): column_piece = lax.all_gather(flat_rows, 'tp', axis=1, tiled=True)  23.3 us
    all_to_all x1, blocking collectives, per_device(): lax.all_to_all(outgoing, 'sp', split_axis=0, concat_axis=0, tiled=True)  23.1 us
    all_gather x1, blocking collectives, per_device(): tag_rows = lax.all_gather(own_tags, 'sp', axis=0, tiled=True)  22.4 us
    reduce_scatter x1, waiting for transfers between devices, per_device(): lax.psum_scatter(lax.dot_general(out_weight, attended, (((0,), (1,)), (()...  20.3 us
    all_to_all x1, waiting for transfers between devices, per_device(): lax.all_to_all(expert_out, 'sp', split_axis=0, concat_axis=0, tiled=True)  16.7 us
    psum x1, blocking collectives, per_device(): squares = lax.psum(jnp.sum(mixed_first * mixed_first, axis=1), 'tp')  5.76 us
  transfers between devices with their start and end apart: 5, of which 5 were waited for; matrix products, arithmetic and copies ran while one was open for 3% of the time, Pallas kernels for 0%

commit v1 on v0

--- a/solution.py
+++ b/solution.py
@@ -9,6 +9,29 @@
 ROTARY_BASE = 10000.0
 CLAMP_LIMIT = 7.0
 SIGMOID_SCALE = 1.702
+
+
+def cut_along(x, dim, size):
+    dims = x.shape
+    blocks = x.reshape(*dims[:dim], size, dims[dim] // size, *dims[dim + 1 :])
+    return jnp.moveaxis(blocks, dim, 0)
+
+
+def laid_out(tiles, dim):
+    tiles = jnp.moveaxis(tiles, 0, dim)
+    shape = tiles.shape
+    return tiles.reshape(*shape[:dim], shape[dim] * shape[dim + 1], *shape[dim + 2 :])
+
+
+def exchange_in_pairs(x, axis, split_dim, concat_dim):
+    devices, index = (lax.axis_size(axis), lax.axis_index(axis))
+    blocks = cut_along(x, split_dim, devices)
+    finished = [blocks[index]]
+    for step in range(1, devices):
+        sent = blocks[index ^ step]
+        finished.append(lax.ppermute(sent, axis, [(i, i ^ step) for i in range(devices)]))
+    blocks = jnp.stack(finished)[index ^ jnp.arange(devices)]
+    return laid_out(blocks, concat_dim)
 
 
 def rope_tables(positions, head_dim):
@@ -179,7 +202,7 @@
     expert_out = lax.psum_scatter(
         partial_value.astype(jnp.bfloat16), "tp", scatter_dimension=2, tiled=True
     )
-    returned = lax.all_to_all(expert_out, "sp", split_axis=0, concat_axis=0, tiled=True)
+    returned = exchange_in_pairs(expert_out, "sp", 0, 0)
     lookup = flat_routes * capacity + slot_index
     picked = (
         returned.reshape(-1, width_local)[lookup]

time: 245 us -> 245 us (level)
  waiting for transfers between devices: 121 us -> 111 us
  starting transfers between devices: 5.82 us -> 11.6 us
  local copies, waits for them, and re-layouts: 14.6 us -> 19.2 us
    all_to_all x1 -> x0, waiting for transfers between devices: 16.7 us -> none  [per_device(): lax.all_to_all(expert_out, 'sp', split_axis=0, concat_axis=0, tiled=True)]
    ppermute x0 -> x7, starting transfers between devices: none -> 11.3 us  [exchange_in_pairs(): lax.ppermute(sent, axis, [(i, i ^ step) for i in range(devices)])]
    ppermute x0 -> x7, waiting for transfers between devices: none -> 6.93 us  [exchange_in_pairs(): lax.ppermute(sent, axis, [(i, i ^ step) for i in range(devices)])]
    all_to_all x1 -> x0, starting transfers between devices: 5.51 us -> none  [per_device(): lax.all_to_all(expert_out, 'sp', split_axis=0, concat_axis=0, tiled=True)]
    unnamed x25 -> x34, local copies, waits for them, and re-layouts: 3.58 us -> 5.34 us
  transfers between devices with their start and end apart: 5 -> 11, of which waited for: 5 -> 5; matrix products, arithmetic and copies ran while one was open for 3% -> 3% of each run, Pallas kernels for 0% -> 0%
where the time goes in v1:
time: 245 us; the launch traced here: 244 us
  waiting for transfers between devices  111 us (45%)
  blocking collectives  51.2 us (21%)
  matrix products  21.6 us (9%)
  local copies, waits for them, and re-layouts  19.2 us (8%)
  other arithmetic  15.9 us (6%)
  between operations  13.7 us (6%)
  starting transfers between devices  11.6 us (5%)
    reduce_scatter x1, waiting for transfers between devices, per_device(): lax.psum_scatter(partial_value.astype(jnp.bfloat16), 'tp', scatter_dimens...  33.9 us
    all_gather x1, waiting for transfers between devices, per_device(): pair_rows = lax.all_gather(stacked, 'sp', axis=0, tiled=True)  26.5 us
    all_gather x1, waiting for transfers between devices, per_device(): column_piece = lax.all_gather(flat_rows, 'tp', axis=1, tiled=True)  23.3 us
    all_to_all x1, blocking collectives, per_device(): lax.all_to_all(outgoing, 'sp', split_axis=0, concat_axis=0, tiled=True)  23.1 us
    all_gather x1, blocking collectives, per_device(): tag_rows = lax.all_gather(own_tags, 'sp', axis=0, tiled=True)  22.4 us
    reduce_scatter x1, waiting for transfers between devices, per_device(): lax.psum_scatter(lax.dot_general(out_weight, attended, (((0,), (1,)), (()...  20.3 us
    ppermute x7, starting transfers between devices, exchange_in_pairs(): lax.ppermute(sent, axis, [(i, i ^ step) for i in range(devices)])  11.3 us
    ppermute x7, waiting for transfers between devices, exchange_in_pairs(): lax.ppermute(sent, axis, [(i, i ^ step) for i in range(devices)])  6.93 us
  transfers between devices with their start and end apart: 11, of which 5 were waited for; matrix products, arithmetic and copies ran while one was open for 3% of the time, Pallas kernels for 0%

profile of v1, /device:TPU:0, one launch (start us, length us, event | category | flops | bytes accessed | tf_op | source)
XLA Modules:
  0.0 244.3 jit_solution(14502426641573958389)
XLA Ops:
  6.5 1.2 copy.40
  12.3 22.4 %all-gather = bf16[8,1,256]{2,1,0:T(2,128)(2,1)S(1)} all-gather(bf16[1,1,256]{2,1,0:T(2,128)(2,1)S(1)} %reshape.421), channel_id=1, replica_groups=mesh['sp'=8,'tp'=4] {'sp'}, dimensions={0}, use_global_device_ids=true | all-gather | bytes 4608 | tf_op jit(solution)/shard_map/all_gather | solution.py:137
  34.7 1.1 copy.42
  38.4 26.5 %all-gather.4.cloned.1.call-done = bf16[2048,512]{0,1:T(8,128)(2,1)} async-done(((bf16[256,512]{0,1:T(8,128)(2,1)}), bf16[2048,512]{0,1:T(8,128)(2,1)}) %all-gather.4.cloned.1.call-update) | async-done | bytes 2097168 | tf_op jit(solution)/shard_map/all_gather | solution.py:136
  64.8 1.7 fusion.47
  66.5 2.6 %fusion = (f32[256,4,2]{0,2,1:T(2,128)S(1)}, f32[4,2048,256,2]{2,1,3,0:T(8,128)S(1)}) fusion(pred[256,2048]{0,1:T(8,128)(4,1)S(1)} %broadcast_compare_fusion, bf16[2048,4,64,1]{0,2,3,1:T(8,128)(2,1)S(1)} %bitcast.139, bf16[256,4,2,64]{0,3,2,1:T(8,128)(2,1)S(1)} %convert_element_type.100), kind=kOutput, calls=%fused_computation.5 | convolution fusion | flops 549451776 | bytes 18620416 | tf_op jit(solution)/shard_map/while/body/eval_jaxpr/tkgd,pkd->tkgp/dot_general | solution.py:79
  69.1 4.0 %fusion.1 = f32[256,4,2]{0,2,1:T(2,128)S(1)} fusion(f32[4,2048,256,2]{2,1,3,0:T(8,128)S(1)} %get-tuple-element.52, f32[256,4,2]{0,2,1:T(2,128)S(1)} %broadcast_maximum_fusion, pred[256,2048]{0,1:T(8,128)(4,1)S(1)} %broadcast_compare_fusion), kind=kLoop, calls=%fused_computation.6 | loop fusion | flops 20969472 | bytes 17317888 | tf_op jit(solution)/shard_map/while/body/eval_jaxpr/reduce_sum | solution.py:87
  73.2 3.9 %fusion.28 = bf16[256,4,2,64]{0,3,2,1:T(8,128)(2,1)S(1)} fusion(bf16[2048,4,64,1]{0,2,3,1:T(8,128)(2,1)S(1)} %bitcast.138, f32[4,2048,256,2]{2,1,3,0:T(8,128)S(1)} %get-tuple-element.52, f32[256,4,2]{0,2,1:T(2,128)S(1)} %broadcast_maximum_fusion, pred[256,2048]{0,1:T(8,128)(4,1)S(1)} %broadcast_compare_fusion, f32[256,4,2]{0,2,1:T(2,128)S(1)} %get-tuple-element.48, ...), kind=kOutput, calls=%fused_computation.27 | convolution fusion | flops 558235648 | bytes 18636800 | tf_op jit(solution)/shard_map/while/body/eval_jaxpr/tkgp,pkd->tkgd/dot_general | solution.py:88
  77.2 1.7 fusion.15
  79.6 1.1 reduce-window.6
  81.8 20.3 %reduce-scatter.3.cloned.1.call-done = bf16[512,256]{0,1:T(8,128)(2,1)} async-done(((bf16[2048,256]{0,1:T(8,128)(2,1)}), bf16[512,256]{0,1:T(8,128)(2,1)}) %reduce-scatter.3.cloned.1.call-update) | async-done | bytes 262160 | tf_op jit(solution)/shard_map/reduce_scatter | solution.py:156
  102.1 1.1 multiply_reduce_fusion.1
  103.2 5.8 %psum.7 = f32[256]{0:T(256)S(1)} all-reduce(f32[256]{0:T(256)S(1)} %multiply_reduce_fusion.1), channel_id=1, replica_groups=mesh['sp'=8,'tp'=4] {'tp'}, use_global_device_ids=true, to_apply=%region_10.11 | all-reduce | flops 256 | bytes 2048 | tf_op jit(solution)/shard_map/psum | solution.py:165
  110.1 2.8 %gather_fusion = bf16[640,512]{1,0:T(8,128)(2,1)S(1)} fusion(bf16[256,512]{1,0:T(8,128)(2,1)S(1)} %multiply_convert_fusion.1, s32[1024]{0:T(1024)S(1)} %pad_clamp_fusion.2), kind=kCustom, calls=%fused_computation | custom fusion | bytes 1313280 | tf_op jit(solution)/shard_map/gather | solution.py:191
  113.0 23.1 %all_to_all.5 = bf16[8,80,512]{2,1,0:T(8,128)(2,1)} all-to-all(bf16[8,80,512]{2,1,0:T(8,128)(2,1)S(1)} %broadcast_select_fusion), channel_id=1, replica_groups=mesh['sp'=8,'tp'=4] {'sp'}, dimensions={0} | all-to-all | bytes 1310720 | tf_op jit(solution)/shard_map/all_to_all | solution.py:192
  136.2 23.3 %all-gather.6.cloned.1.call-done = bf16[640,2048]{1,0:T(8,128)(2,1)} async-done(((bf16[640,512]{1,0:T(8,128)(2,1)}), bf16[640,2048]{1,0:T(8,128)(2,1)}) %all-gather.6.cloned.1.call-update) | async-done | bytes 2621456 | tf_op jit(solution)/shard_map/all_gather | solution.py:195
  159.5 5.6 %fusion.8 = f32[640,1024]{1,0:T(8,128)S(1)} fusion(bf16[640,2048]{1,0:T(8,128)(2,1)} %all-gather.6.cloned.1.call-done, bf16[1,2048,1024]{2,1,0:T(8,128)(2,1)} %param.26), kind=kOutput, calls=%fused_computation.12 | convolution fusion | flops 2684354560 | bytes 9437184 | tf_op jit(solution)/shard_map/dot_general | solution.py:197
  165.1 3.5 %multiply_convert_fusion = bf16[640,1024]{1,0:T(8,128)(2,1)S(1)} fusion(f32[640,1024]{1,0:T(8,128)S(1)} %fusion.8, bf16[640,2048]{1,0:T(8,128)(2,1)S(1)} %copy-done.9, bf16[1,2048,1024]{2,1,0:T(8,128)(2,1)S(1)} %copy-done.7), kind=kOutput, calls=%fused_computation.17 | convolution fusion | flops 2690908160 | bytes 10747904 | tf_op jit(solution)/shard_map/dot_general | solution.py:196
  168.7 4.2 %fusion.12 = bf16[8,80,2048]{2,1,0:T(8,128)(2,1)} fusion(bf16[8,80,1024]{2,1,0:T(8,128)(2,1)S(1)} %bitcast.146, bf16[1,1024,2048]{2,1,0:T(8,128)(2,1)S(1)} %copy-done.8), kind=kOutput, calls=%fused_computation.16 | convolution fusion | flops 2685665280 | bytes 8126464 | tf_op jit(solution)/shard_map/dot_general | solution.py:199
  173.5 33.9 %reduce-scatter.5.cloned.1.call-done = bf16[8,80,512]{2,1,0:T(8,128)(2,1)} async-done(((bf16[8,80,2048]{2,1,0:T(8,128)(2,1)}), bf16[8,80,512]{2,1,0:T(8,128)(2,1)}) %reduce-scatter.5.cloned.1.call-update) | async-done | bytes 655376 | tf_op jit(solution)/shard_map/reduce_scatter | solution.py:202
  207.4 1.2 constant_dynamic-slice_fusion
  208.6 1.5 collective-permute-start
  210.1 1.5 collective-permute-start.1
  212.1 2.4 collective-permute-start.3
  214.5 1.4 collective-permute-start.4
  216.9 3.4 %collective-permute-start.5 = (bf16[1,80,512]{2,1,0:T(8,128)(2,1)S(1)}, bf16[1,80,512]{2,1,0:T(8,128)(2,1)S(1)}, u32[]{:S(2)}, u32[]{:S(2)}) collective-permute-start(bf16[1,80,512]{2,1,0:T(8,128)(2,1)S(1)} %get-tuple-element.24), channel_id=1, source_target_pairs={{0,24},{4,28},{8,16},{12,20},{16,8},{20,12},{24,0},{28,4},{1,25},{... | collective-permute-start | bytes 245768 | tf_op jit(solution)/shard_map/ppermute | solution.py:32
  220.9 6.9 %collective-permute-done.4 = bf16[1,80,512]{2,1,0:T(8,128)(2,1)S(1)} collective-permute-done((bf16[1,80,512]{2,1,0:T(8,128)(2,1)S(1)}, bf16[1,80,512]{2,1,0:T(8,128)(2,1)S(1)}, u32[]{:S(2)}, u32[]{:S(2)}) %collective-permute-start.4) | collective-permute-done | bytes 81952 | tf_op jit(solution)/shard_map/ppermute | solution.py:32
  228.7 1.7 gather_fusion.1
  230.4 2.6 %gather_fusion.2 = bf16[512,512]{1,0:T(8,128)(2,1)} fusion(bf16[640,512]{1,0:T(8,128)(2,1)S(1)} %bitcast.135, s32[1024]{0:T(1024)S(1)} %pad_clamp_fusion), kind=kCustom, calls=%fused_computation.2 | custom fusion | bytes 1050624 | tf_op jit(solution)/shard_map/gather | solution.py:208
  233.0 1.7 reshape.392
  234.7 1.3 multiply_reduce_fusion
  236.0 1.8 add_convert_fusion
  (99 shorter events, 13.3 us)
Async XLA Ops:
  6.5 70.7 %copy-start = (bf16[512,2048]{1,0:T(8,128)(2,1)S(1)}, bf16[512,2048]{1,0:T(8,128)(2,1)}, u32[]{:S(2)}) copy-start(bf16[512,2048]{1,0:T(8,128)(2,1)} %param.20) | copy-start | bytes 6291460
  6.5 29.6 %copy-start.6 = (f32[64]{0:T(128)S(1)}, f32[64]{0:T(128)}, u32[]{:S(2)}) copy-start(f32[64]{0:T(128)} %param.18) | copy-start | bytes 772
  6.5 58.3 %all-gather.4.cloned.1.call-start = ((), (), s32[]{:S(2)}) async-start(), calls=%async_computation.3 | async-start | bytes 2359296 | tf_op jit(solution)/shard_map/all_gather | solution.py:136
  11.6 90.5 %reduce-scatter.3.cloned.1.call-start = ((), (), s32[]{:S(2)}) async-start(), calls=%async_computation.4 | async-start | bytes 1310720 | tf_op jit(solution)/shard_map/reduce_scatter | solution.py:156
  77.2 2.0 copy-start.3
  77.2 24.9 %copy-start.1 = (bf16[256,512]{1,0:T(8,128)(2,1)S(1)}, bf16[256,512]{1,0:T(8,128)(2,1)}, u32[]{:S(2)}) copy-start(bf16[256,512]{1,0:T(8,128)(2,1)} %param.21) | copy-start | bytes 786436
  77.2 31.8 %copy-start.4 = (f32[512]{0:T(512)S(1)}, f32[512]{0:T(512)}, u32[]{:S(2)}) copy-start(f32[512]{0:T(512)} %param.22) | copy-start | bytes 6148
  78.9 80.6 %all-gather.6.cloned.1.call-start = ((), (), s32[]{:S(2)}) async-start(), calls=%async_computation.5 | async-start | bytes 3276800 | tf_op jit(solution)/shard_map/all_gather | solution.py:195
  136.1 71.3 %reduce-scatter.5.cloned.1.call-start = ((), (), s32[]{:S(2)}) async-start(), calls=%async_computation.6 | async-start | bytes 3276800 | tf_op jit(solution)/shard_map/reduce_scatter | solution.py:202
  159.5 5.6 %copy-start.7 = (bf16[1,2048,1024]{2,1,0:T(8,128)(2,1)S(1)}, bf16[1,2048,1024]{2,1,0:T(8,128)(2,1)}, u32[]{:S(2)}) copy-start(bf16[1,2048,1024]{2,1,0:T(8,128)(2,1)} %param.25) | copy-start | bytes 12582916
  159.5 5.6 %copy-start.9 = (bf16[640,2048]{1,0:T(8,128)(2,1)S(1)}, bf16[640,2048]{1,0:T(8,128)(2,1)}, u32[]{:S(2)}) copy-start(bf16[640,2048]{1,0:T(8,128)(2,1)} %all-gather.6.cloned.1.call-done) | copy-start | bytes 7864324
  165.1 3.6 %copy-start.8 = (bf16[1,1024,2048]{2,1,0:T(8,128)(2,1)S(1)}, bf16[1,1024,2048]{2,1,0:T(8,128)(2,1)}, u32[]{:S(2)}) copy-start(bf16[1,1024,2048]{2,1,0:T(8,128)(2,1)} %param.27) | copy-start | bytes 12582916
  168.7 4.5 %copy-start.5 = (f32[256,2]{0,1:T(2,128)S(1)}, f32[256,2]{0,1:T(2,128)}, u32[]{:S(2)}) copy-start(f32[256,2]{0,1:T(2,128)} %param.24) | copy-start | bytes 6148
  208.6 8.3 %collective-permute-start = (bf16[1,80,512]{2,1,0:T(8,128)(2,1)S(1)}, bf16[1,80,512]{2,1,0:T(8,128)(2,1)S(1)}, u32[]{:S(2)}, u32[]{:S(2)}) collective-permute-start(bf16[1,80,512]{2,1,0:T(8,128)(2,1)S(1)} %get-tuple-element.40), channel_id=1, source_target_pairs={{0,4},{4,0},{8,12},{12,8},{16,20},{20,16},{24,28},{28,24},{1,5},{5... | collective-permute-start | bytes 245768 | tf_op jit(solution)/shard_map/ppermute | solution.py:32
  210.1 10.2 %collective-permute-start.1 = (bf16[1,80,512]{2,1,0:T(8,128)(2,1)S(1)}, bf16[1,80,512]{2,1,0:T(8,128)(2,1)S(1)}, u32[]{:S(2)}, u32[]{:S(2)}) collective-permute-start(bf16[1,80,512]{2,1,0:T(8,128)(2,1)S(1)} %get-tuple-element.38), channel_id=1, source_target_pairs={{0,8},{4,12},{8,0},{12,4},{16,24},{20,28},{24,16},{28,20},{1,9},{5... | collective-permute-start | bytes 245768 | tf_op jit(solution)/shard_map/ppermute | solution.py:32
  211.6 9.2 %collective-permute-start.2 = (bf16[1,80,512]{2,1,0:T(8,128)(2,1)S(1)}, bf16[1,80,512]{2,1,0:T(8,128)(2,1)S(1)}, u32[]{:S(2)}, u32[]{:S(2)}) collective-permute-start(bf16[1,80,512]{2,1,0:T(8,128)(2,1)S(1)} %get-tuple-element.36), channel_id=1, source_target_pairs={{0,12},{4,8},{8,4},{12,0},{16,28},{20,24},{24,20},{28,16},{1,13},{... | collective-permute-start | bytes 245768 | tf_op jit(solution)/shard_map/ppermute | solution.py:32
  212.1 8.7 %collective-permute-start.3 = (bf16[1,80,512]{2,1,0:T(8,128)(2,1)S(1)}, bf16[1,80,512]{2,1,0:T(8,128)(2,1)S(1)}, u32[]{:S(2)}, u32[]{:S(2)}) collective-permute-start(bf16[1,80,512]{2,1,0:T(8,128)(2,1)S(1)} %get-tuple-element.26), channel_id=1, source_target_pairs={{0,16},{4,20},{8,24},{12,28},{16,0},{20,4},{24,8},{28,12},{1,17},{... | collective-permute-start | bytes 245768 | tf_op jit(solution)/shard_map/ppermute | solution.py:32
  214.5 13.3 %collective-permute-start.4 = (bf16[1,80,512]{2,1,0:T(8,128)(2,1)S(1)}, bf16[1,80,512]{2,1,0:T(8,128)(2,1)S(1)}, u32[]{:S(2)}, u32[]{:S(2)}) collective-permute-start(bf16[1,80,512]{2,1,0:T(8,128)(2,1)S(1)} %get-tuple-element.25), channel_id=1, source_target_pairs={{0,20},{4,16},{8,28},{12,24},{16,4},{20,0},{24,12},{28,8},{1,21},{... | collective-permute-start | bytes 245768 | tf_op jit(solution)/shard_map/ppermute | solution.py:32
  216.9 10.9 %collective-permute-start.5 = (bf16[1,80,512]{2,1,0:T(8,128)(2,1)S(1)}, bf16[1,80,512]{2,1,0:T(8,128)(2,1)S(1)}, u32[]{:S(2)}, u32[]{:S(2)}) collective-permute-start(bf16[1,80,512]{2,1,0:T(8,128)(2,1)S(1)} %get-tuple-element.24), channel_id=1, source_target_pairs={{0,24},{4,28},{8,16},{12,20},{16,8},{20,12},{24,0},{28,4},{1,25},{... | collective-permute-start | bytes 245768 | tf_op jit(solution)/shard_map/ppermute | solution.py:32
  220.3 7.6 %collective-permute-start.6 = (bf16[1,80,512]{2,1,0:T(8,128)(2,1)S(1)}, bf16[1,80,512]{2,1,0:T(8,128)(2,1)S(1)}, u32[]{:S(2)}, u32[]{:S(2)}) collective-permute-start(bf16[1,80,512]{2,1,0:T(8,128)(2,1)S(1)} %get-tuple-element.23), channel_id=1, source_target_pairs={{0,28},{4,24},{8,20},{12,16},{16,12},{20,8},{24,4},{28,0},{1,29},{... | collective-permute-start | bytes 245768 | tf_op jit(solution)/shard_map/ppermute | solution.py:32
  227.9 0.8 copy-start.2
Sparse Core Ops, SparseCore 0:
  11.7 53.0 all-gather.3
  79.1 22.9 reduce-scatter.2
  136.2 23.2 all-gather.5
  173.0 34.3 reduce-scatter.4
